TPU v7x, 32 devices: a whole 2x2x4 slice. The times are simulated.
32 devices in a mesh: fs: 16 (over z, y, x), tp: 2 (over core).
Axes of the slice: x: 2, y: 2, z: 4, core: 2. Of those that a mesh axis runs over, the one named last changes fastest.
Arguments:
- sequence_entries: bfloat16 [4096, 2048], P('fs', 'tp'), may hold values from -6 to 6
- former_norm_factor: float32 [2048], replicated, may hold values from 0.1 to 1.9
- conveyor_matrix: float32 [2048, 1536], P('fs', 'tp'), may hold values from -0.125 to 0.125
- conveyor_rescalers: float32 [1536], P('tp'), may hold values from 0.3 to 3
- blend_value_matrix: float32 [2048, 1536], P('fs', 'tp'), may hold values from -0.125 to 0.125
- blend_rescalers: float32 [1536], P('tp'), may hold values from 0.18 to 4.8, as said below
- blend_norm_factor: float32 [1536], P('tp'), may hold values from 0.1 to 1.9
- location_matrices: bfloat16 [24, 128, 128], P('tp'), may hold values from -0.5 to 0.5
- location_offsets: float32 [24, 128], P('tp'), may hold values from 0.1 to 1.9
- branch_emission_matrix: float32 [1536, 2048], P('tp', 'fs'), may hold values from -0.15625 to 0.15625
- emission_rescalers: float32 [2048], P('fs'), may hold values from 0.3 to 3
- latter_norm_factor: float32 [2048], replicated, may hold values from 0.1 to 1.9
- valve_matrix: float32 [2048, 5632], P('fs', 'tp'), may hold values from -0.125 to 0.125
- valve_rescalers: float32 [5632], P('tp'), may hold values from 0.3 to 3
- raising_matrix: float32 [2048, 5632], P('fs', 'tp'), may hold values from -0.125 to 0.125
- raising_rescalers: float32 [5632], P('tp'), may hold values from 0.3 to 3
- lowering_matrix: float32 [5632, 2048], P('tp', 'fs'), may hold values from -0.078125 to 0.078125
- lowering_rescalers: float32 [2048], P('fs'), may hold values from 0.3 to 3
Outputs:
- layer_out: bfloat16 [4096, 2048], P('fs', 'tp')
Inputs may be any that keep to these rules, and one draw needn't show every extreme that they name: `blend_rescalers`: positive column scales.
All inputs are finite; a program needn't handle non-finite values.
Results may differ from a plain program's by a relative error of at most 0.02.
Values may be sent and summed in bfloat16 or wider, within the bound.
A program may use at most 128 MiB of HBM per device.

v0:
```python
import jax
import jax.numpy as jnp
from jax import lax
from jax.sharding import PartitionSpec as P

EPS = 1e-06


def normalize(rows, gain):
    values = rows.astype(jnp.float32)
    factor = lax.rsqrt(jnp.mean(values * values, axis=-1, keepdims=True) + EPS)
    return (values * factor * gain).astype(jnp.bfloat16)


def elementwise_plus(left_rows, pieces):
    return (
        jnp.dot(left_rows, pieces[0], preferred_element_type=jnp.float32),
        jnp.dot(left_rows, pieces[1], preferred_element_type=jnp.float32),
    )


def project_cols(left_rows, scales, piece):
    return jnp.dot(left_rows, piece, preferred_element_type=jnp.float32) * scales


def on_device(
    sequence_entries,
    former_norm_factor,
    conveyor_matrix,
    conveyor_rescalers,
    blend_value_matrix,
    blend_rescalers,
    blend_norm_factor,
    location_matrices,
    location_offsets,
    branch_emission_matrix,
    emission_rescalers,
    latter_norm_factor,
    valve_matrix,
    valve_rescalers,
    raising_matrix,
    raising_rescalers,
    lowering_matrix,
    lowering_rescalers,
):
    out_scales, down_scales = (
        lax.all_gather(emission_rescalers, "fs", axis=0, tiled=True),
        lax.all_gather(lowering_rescalers, "fs", axis=0, tiled=True),
    )
    full_rows = lax.all_gather(sequence_entries, "tp", axis=1, tiled=True)
    own_width = sequence_entries.shape[1]
    own_start = lax.axis_index("tp") * own_width
    standardized_source = normalize(full_rows, former_norm_factor)
    conveyor_prior, stream_prior = elementwise_plus(
        standardized_source,
        (
            lax.all_gather(conveyor_matrix.astype(jnp.bfloat16), "fs", axis=0, tiled=True),
            lax.all_gather(blend_value_matrix.astype(jnp.bfloat16), "fs", axis=0, tiled=True),
        ),
    )
    conveyor_current = jax.nn.gelu(conveyor_prior * conveyor_rescalers)
    signal = jax.nn.gelu(stream_prior * blend_rescalers)
    total_sq = lax.psum(jnp.sum(signal * signal, axis=1), "tp")
    channels = signal.shape[1] * lax.axis_size("tp")
    signal_norm = (
        signal * lax.rsqrt(total_sq / channels + EPS)[:, None] * blend_norm_factor
    ).astype(jnp.bfloat16)
    local_groups = location_matrices.shape[0]
    block_len = location_matrices.shape[1]
    group_width = signal.shape[1] // local_groups
    lower_mask = jnp.tril(jnp.ones((block_len, block_len), bool))
    masked = jnp.where(lower_mask[None], location_matrices, jnp.zeros((), jnp.bfloat16))
    signal_blocks = signal_norm.reshape(-1, block_len, local_groups, group_width)
    location_blended = jnp.einsum(
        "gts,bsgd->btgd", masked, signal_blocks, preferred_element_type=jnp.float32
    )
    location_blended = location_blended + location_offsets.T[None, :, :, None]
    filtered_result = (conveyor_current * location_blended.reshape(conveyor_current.shape)).astype(
        jnp.bfloat16
    )
    mixer_terms = project_cols(
        filtered_result,
        out_scales,
        lax.all_gather(branch_emission_matrix.astype(jnp.bfloat16), "fs", axis=1, tiled=True),
    )
    summed = lax.psum(mixer_terms.astype(jnp.bfloat16), "tp").astype(jnp.float32)
    mid_rows = (full_rows.astype(jnp.float32) + summed).astype(jnp.bfloat16)
    mid_own = lax.dynamic_slice_in_dim(mid_rows, own_start, own_width, 1)
    ffn_in = normalize(mid_rows, latter_norm_factor)
    gate_half = valve_matrix.astype(jnp.bfloat16)
    up_half = raising_matrix.astype(jnp.bfloat16)
    whole_gate, whole_up = (
        lax.all_gather(gate_half, "fs", axis=0, tiled=True),
        lax.all_gather(up_half, "fs", axis=0, tiled=True),
    )
    pre_gate = jnp.dot(ffn_in, whole_gate, preferred_element_type=jnp.float32)
    pre_up = jnp.dot(ffn_in, whole_up, preferred_element_type=jnp.float32)
    hidden = (jax.nn.silu(pre_gate * valve_rescalers) * (pre_up * raising_rescalers)).astype(
        jnp.bfloat16
    )
    ffn_terms = project_cols(
        hidden,
        down_scales,
        lax.all_gather(lowering_matrix.astype(jnp.bfloat16), "fs", axis=1, tiled=True),
    )
    ffn_share = lax.psum_scatter(
        ffn_terms.astype(jnp.bfloat16), "tp", scatter_dimension=1, tiled=True
    ).astype(jnp.float32)
    return (mid_own.astype(jnp.float32) + ffn_share).astype(jnp.bfloat16)


def solution(mesh):
    return jax.shard_map(
        on_device,
        mesh=mesh,
        in_specs=(
            P("fs", "tp"),
            P(),
            P("fs", "tp"),
            P("tp"),
            P("fs", "tp"),
            P("tp"),
            P("tp"),
            P("tp", None, None),
            P("tp", None),
            P("tp", "fs"),
            P("fs"),
            P(),
            P("fs", "tp"),
            P("tp"),
            P("fs", "tp"),
            P("tp"),
            P("tp", "fs"),
            P("fs"),
        ),
        out_specs=P("fs", "tp"),
        check_vma=False,
    )
```

profile of v0, /device:TPU:0, one launch (start us, length us, event | category | flops | bytes accessed | tf_op | source)
XLA Modules:
  0.0 764.5 jit_solution(3299104337699982424)
XLA Ops:
  6.5 0.7 all-gather.10.cloned.1.call-update
  7.3 1.7 convert_element_type.64
  9.1 1.7 convert_element_type.63
  10.8 0.0 all-gather.16.cloned.1.call-start
  10.9 1.7 convert_element_type.67
  12.6 42.5 %all-gather = f32[16,1,128]{2,1,0:T(1,128)S(1)} all-gather(f32[1,1,128]{2,1,0:T(1,128)S(1)} %bitcast.34), channel_id=1, replica_groups=mesh['fs'=16,'tp'=2] {'fs'}, dimensions={0}, use_global_device_ids=true | all-gather | bytes 8704 | tf_op jit(solution)/shard_map/all_gather | solution.py:47
  55.1 1.5 fusion.7
  56.7 35.8 %all-gather.14.cloned.1.call-done = bf16[2048,768]{1,0:T(8,128)(2,1)} async-done(((bf16[128,768]{1,0:T(8,128)(2,1)}), bf16[2048,768]{1,0:T(8,128)(2,1)}) %all-gather.14.cloned.1.call-update) | async-done | bytes 3145744 | tf_op jit(solution)/shard_map/all_gather | solution.py:58
  92.5 3.5 multiply_reduce_fusion
  96.0 2.6 psum.14
  98.6 0.1 multiply_convert_fusion
  98.8 0.2 copy.25
  99.0 0.1 reshape.40
  99.1 0.4 fusion.11
  99.5 0.6 copy.27
  100.1 0.1 copy.34
  100.2 0.3 copy.28
  100.4 61.3 %all-gather.12.cloned.1.call-done = bf16[2048,768]{1,0:T(8,128)(2,1)} async-done(((bf16[128,768]{1,0:T(8,128)(2,1)}), bf16[2048,768]{1,0:T(8,128)(2,1)}) %all-gather.12.cloned.1.call-update) | async-done | bytes 3145744 | tf_op jit(solution)/shard_map/all_gather | solution.py:57
  161.7 77.2 %all-gather.16.cloned.1.call-done = bf16[768,2048]{1,0:T(8,128)(2,1)} async-done(((bf16[768,128]{1,0:T(8,128)(2,1)}), bf16[768,2048]{1,0:T(8,128)(2,1)}) %all-gather.16.cloned.1.call-update) | async-done | bytes 3145744 | tf_op jit(solution)/shard_map/all_gather | solution.py:84
  238.9 6.2 fusion.3
  245.2 1.0 convert_element_type.74
  246.2 2.4 convert_element_type.75
  248.7 0.9 convert_element_type.77
  249.8 38.3 %all-gather.1 = f32[16,1,128]{2,1,0:T(1,128)S(1)} all-gather(f32[1,1,128]{2,1,0:T(1,128)S(1)} %bitcast.35), channel_id=1, replica_groups=mesh['fs'=16,'tp'=2] {'fs'}, dimensions={0}, use_global_device_ids=true | all-gather | bytes 8704 | tf_op jit(solution)/shard_map/all_gather | solution.py:48
  288.0 1.7 fusion.4
  289.8 118.3 %all-gather.18.cloned.1.call-done = bf16[2048,2816]{1,0:T(8,128)(2,1)} async-done(((bf16[128,2816]{1,0:T(8,128)(2,1)}), bf16[2048,2816]{1,0:T(8,128)(2,1)}) %all-gather.18.cloned.1.call-update) | async-done | bytes 11534352 | tf_op jit(solution)/shard_map/all_gather | solution.py:93
  408.1 9.1 %convolution_multiply_fusion.1 = f32[256,2816]{1,0:T(8,128)} fusion(bf16[2048,2816]{1,0:T(8,128)(2,1)} %all-gather.18.cloned.1.call-done, f32[2816]{0:T(1024)S(1)} %copy-done.8, bf16[256,2048]{1,0:T(8,128)(2,1)S(1)} %get-tuple-element.6, f32[2048]{0:T(1024)S(1)} %copy-done.11, f32[256]{0:T(256)S(1)} %add_rsqrt_fusion), kind=kOutput, calls=%fused_computation.2 | convolution fusion | flops 2955608064 | bytes 15486976 | tf_op jit(solution)/shard_map/dot_general | solution.py:96
  417.3 133.3 %all-gather.20.cloned.1.call-done = bf16[2048,2816]{1,0:T(8,128)(2,1)} async-done(((bf16[128,2816]{1,0:T(8,128)(2,1)}), bf16[2048,2816]{1,0:T(8,128)(2,1)}) %all-gather.20.cloned.1.call-update) | async-done | bytes 11534352 | tf_op jit(solution)/shard_map/all_gather | solution.py:94
  550.5 183.0 %all-gather.22.cloned.1.call-done = bf16[2816,2048]{1,0:T(8,128)(2,1)} async-done(((bf16[2816,128]{1,0:T(8,128)(2,1)}), bf16[2816,2048]{1,0:T(8,128)(2,1)}) %all-gather.22.cloned.1.call-update) | async-done | bytes 11534352 | tf_op jit(solution)/shard_map/all_gather | solution.py:104
  733.5 15.7 %fusion.2 = bf16[256,2048]{1,0:T(8,128)(2,1)} fusion(bf16[2816,2048]{1,0:T(8,128)(2,1)} %all-gather.22.cloned.1.call-done, f32[2048]{0:T(1024)S(1)} %bitcast.33, bf16[2048,2816]{1,0:T(8,128)(2,1)} %all-gather.20.cloned.1.call-done, f32[256,2816]{1,0:T(8,128)} %convolution_multiply_fusion.1, f32[2816]{0:T(1024)S(1)} %copy-done.9, ...), kind=kOutput, calls=%fused_computation.11 | convolution fusion | flops 5913772032 | bytes 28078080 | tf_op jit(solution)/shard_map/dot_general | solution.py:23
  749.2 6.7 reduce-scatter.2.cloned.1.call-done
  755.9 2.0 add_convert_fusion
  (50 shorter events, 0.6 us)
Async XLA Ops:
  6.5 6.1 copy-start.6
  6.5 86.0 %copy-start.10 = (f32[2048]{0:T(1024)S(1)}, f32[2048]{0:T(1024)}, u32[]{:S(2)}) copy-start(f32[2048]{0:T(1024)} %param.19) | copy-start | bytes 24580
  6.5 86.0 %copy-start.12 = (f32[768]{0:T(1024)S(1)}, f32[768]{0:T(1024)}, u32[]{:S(2)}) copy-start(f32[768]{0:T(1024)} %param.23) | copy-start | bytes 9220
  6.5 48.6 %all-gather.10.cloned.1.call-start = ((), (), s32[]{:S(2)}) async-start(), calls=%async_computation.1 | async-start | bytes 1572864 | tf_op jit(solution)/shard_map/all_gather | solution.py:50
  7.3 85.3 %all-gather.14.cloned.1.call-start = ((), (), s32[]{:S(2)}) async-start(), calls=%async_computation.3 | async-start | bytes 3342336 | tf_op jit(solution)/shard_map/all_gather | solution.py:58
  9.0 152.7 %all-gather.12.cloned.1.call-start = ((), (), s32[]{:S(2)}) async-start(), calls=%async_computation.2 | async-start | bytes 3342336 | tf_op jit(solution)/shard_map/all_gather | solution.py:57
  10.8 228.1 %all-gather.16.cloned.1.call-start = ((), (), s32[]{:S(2)}) async-start(), calls=%async_computation.4 | async-start | bytes 3342336 | tf_op jit(solution)/shard_map/all_gather | solution.py:84
  12.6 275.5 %all-reduce.2.cloned.1.call-start = ((), (), s32[]{:S(2)}) async-start(), calls=%async_computation.5 | async-start | bytes 2097152 | tf_op jit(solution)/shard_map/psum | solution.py:86
  56.7 42.0 %copy-start.5 = (f32[768]{0:T(1024)S(1)}, f32[768]{0:T(1024)}, u32[]{:S(2)}) copy-start(f32[768]{0:T(1024)} %param.24) | copy-start | bytes 9220
  56.7 42.4 %copy-start.4 = (f32[12,128]{1,0:T(8,128)S(1)}, f32[12,128]{1,0:T(8,128)}, u32[]{:S(2)}) copy-start(f32[12,128]{1,0:T(8,128)} %param.26) | copy-start | bytes 18436
  96.0 3.1 copy-start.3
  99.1 139.8 %copy-start = (bf16[256,2048]{1,0:T(8,128)(2,1)S(1)}, bf16[256,2048]{1,0:T(8,128)(2,1)}, u32[]{:S(2)}) copy-start(bf16[256,2048]{1,0:T(8,128)(2,1)} %all-gather.10.cloned.1.call-done) | copy-start | bytes 3145732
  99.1 139.8 %copy-start.13 = (f32[768]{0:T(1024)S(1)}, f32[768]{0:T(1024)}, u32[]{:S(2)}) copy-start(f32[768]{0:T(1024)} %param.21) | copy-start | bytes 9220
  238.9 6.2 copy-start.1
  245.1 163.0 %all-gather.18.cloned.1.call-start = ((), (), s32[]{:S(2)}) async-start(), calls=%async_computation.6 | async-start | bytes 12255232 | tf_op jit(solution)/shard_map/all_gather | solution.py:93
  246.1 2.6 copy-start.2
  246.2 3.6 copy-start.7
  246.2 304.4 %all-gather.20.cloned.1.call-start = ((), (), s32[]{:S(2)}) async-start(), calls=%async_computation.7 | async-start | bytes 12255232 | tf_op jit(solution)/shard_map/all_gather | solution.py:94
  248.6 159.5 %copy-start.8 = (f32[2816]{0:T(1024)S(1)}, f32[2816]{0:T(1024)}, u32[]{:S(2)}) copy-start(f32[2816]{0:T(1024)} %param.31) | copy-start | bytes 33796
  248.7 159.5 %copy-start.11 = (f32[2048]{0:T(1024)S(1)}, f32[2048]{0:T(1024)}, u32[]{:S(2)}) copy-start(f32[2048]{0:T(1024)} %param.29) | copy-start | bytes 24580
  248.7 484.8 %all-gather.22.cloned.1.call-start = ((), (), s32[]{:S(2)}) async-start(), calls=%async_computation.8 | async-start | bytes 12255232 | tf_op jit(solution)/shard_map/all_gather | solution.py:104
  249.7 506.2 %reduce-scatter.2.cloned.1.call-start = ((), (), s32[]{:S(2)}) async-start(), calls=%async_computation.9 | async-start | bytes 1572864 | tf_op jit(solution)/shard_map/reduce_scatter | solution.py:106
  408.1 325.4 %copy-start.9 = (f32[2816]{0:T(1024)S(1)}, f32[2816]{0:T(1024)}, u32[]{:S(2)}) copy-start(f32[2816]{0:T(1024)} %param.33) | copy-start | bytes 33796
Sparse Core Ops, SparseCore 0:
  8.9 11.7 all-gather.9
  23.4 69.0 all-gather.13
  95.3 66.3 all-gather.11
  164.3 74.5 all-gather.15
  245.2 17.5 all-reduce.1
  265.5 142.6 all-gather.17
  410.9 139.6 all-gather.19
  553.2 180.2 all-gather.21
  749.3 6.5 reduce-scatter.1
where the time goes:
time: 765 us; the launch traced here: 764 us
  waiting for transfers between devices  616 us (81%)
  blocking collectives  83.3 us (11%)
  matrix products  34.8 us (5%)
  other arithmetic  14.9 us (2%)
  between operations  13.4 us (2%)
    all_gather x1, waiting for transfers between devices, on_device(): lax.all_gather(lowering_matrix.astype(jnp.bfloat16), 'fs', axis=1, tiled=...  183 us
    all_gather x1, waiting for transfers between devices, on_device(): lax.all_gather(up_half, 'fs', axis=0, tiled=True)  133 us
    all_gather x1, waiting for transfers between devices, on_device(): lax.all_gather(gate_half, 'fs', axis=0, tiled=True)  118 us
    all_gather x1, waiting for transfers between devices, on_device(): lax.all_gather(branch_emission_matrix.astype(jnp.bfloat16), 'fs', axis=1,...  77.2 us
    all_gather x1, waiting for transfers between devices, on_device(): lax.all_gather(conveyor_matrix.astype(jnp.bfloat16), 'fs', axis=0, tiled=...  61.3 us
    all_gather x1, blocking collectives, on_device(): lax.all_gather(emission_rescalers, 'fs', axis=0, tiled=True)  42.5 us
    all_gather x1, blocking collectives, on_device(): lax.all_gather(lowering_rescalers, 'fs', axis=0, tiled=True)  38.3 us
    all_gather x1, waiting for transfers between devices, on_device(): lax.all_gather(blend_value_matrix.astype(jnp.bfloat16), 'fs', axis=0, til...  35.8 us
  transfers between devices with their start and end apart: 9, of which 7 were waited for; matrix products, arithmetic and copies ran while one was open for 4% of the time, Pallas kernels for 0%

commit v1 on v0

--- a/solution.py
+++ b/solution.py
@@ -101,7 +101,7 @@
     ffn_terms = project_cols(
         hidden,
         down_scales,
-        lax.all_gather(lowering_matrix.astype(jnp.bfloat16), "fs", axis=1, tiled=True),
+        jnp.concatenate(lax.all_gather(lowering_matrix.astype(jnp.bfloat16), "fs"), axis=1),
     )
     ffn_share = lax.psum_scatter(
         ffn_terms.astype(jnp.bfloat16), "tp", scatter_dimension=1, tiled=True

time: 765 us -> 725 us (0.948)
  waiting for transfers between devices: 616 us -> 561 us
  local copies, waits for them, and re-layouts: 1.27 us -> 16.4 us
    all_gather x1, waiting for transfers between devices: 183 us -> 118 us  [on_device(): lax.all_gather(lowering_matrix.astype(jnp.bfloat16), 'fs')]
    reshape x0 -> x1, local copies, waits for them, and re-layouts: none -> 15.2 us  [on_device(): jnp.concatenate(lax.all_gather(lowering_matrix.astype(jnp.bfloat16), 'fs'...]
    all_gather x1, waiting for transfers between devices: 118 us -> 127 us  [on_device(): lax.all_gather(gate_half, 'fs', axis=0, tiled=True)]
  transfers between devices with their start and end apart: 9 -> 9, of which waited for: 7 -> 7; matrix products, arithmetic and copies ran while one was open for 4% -> 6% of each run, Pallas kernels for 0% -> 0%
where the time goes in v1:
time: 725 us; the launch traced here: 724 us
  waiting for transfers between devices  561 us (77%)
  blocking collectives  83.3 us (11%)
  matrix products  34.8 us (5%)
  local copies, waits for them, and re-layouts  16.4 us (2%)
  other arithmetic  14.9 us (2%)
  between operations  13.4 us (2%)
    all_gather x1, waiting for transfers between devices, on_device(): lax.all_gather(up_half, 'fs', axis=0, tiled=True)  133 us
    all_gather x1, waiting for transfers between devices, on_device(): lax.all_gather(gate_half, 'fs', axis=0, tiled=True)  127 us
    all_gather x1, waiting for transfers between devices, on_device(): lax.all_gather(lowering_matrix.astype(jnp.bfloat16), 'fs')  118 us
    all_gather x1, waiting for transfers between devices, on_device(): lax.all_gather(branch_emission_matrix.astype(jnp.bfloat16), 'fs', axis=1,...  77.2 us
    all_gather x1, waiting for transfers between devices, on_device(): lax.all_gather(conveyor_matrix.astype(jnp.bfloat16), 'fs', axis=0, tiled=...  61.3 us
    all_gather x1, blocking collectives, on_device(): lax.all_gather(emission_rescalers, 'fs', axis=0, tiled=True)  42.5 us
    all_gather x1, blocking collectives, on_device(): lax.all_gather(lowering_rescalers, 'fs', axis=0, tiled=True)  38.3 us
    all_gather x1, waiting for transfers between devices, on_device(): lax.all_gather(blend_value_matrix.astype(jnp.bfloat16), 'fs', axis=0, til...  35.8 us
  transfers between devices with their start and end apart: 9, of which 7 were waited for; matrix products, arithmetic and copies ran while one was open for 6% of the time, Pallas kernels for 0%

profile of v1, /device:TPU:0, one launch (start us, length us, event | category | flops | bytes accessed | tf_op | source)
XLA Modules:
  0.0 723.9 jit_solution(17273863778185249813)
XLA Ops:
  6.5 0.7 all-gather.11.cloned.1.call-update
  7.3 1.7 convert_element_type.64
  9.1 1.7 convert_element_type.63
  10.9 1.7 convert_element_type.67
  12.6 42.5 %all-gather.1 = f32[16,1,128]{2,1,0:T(1,128)S(1)} all-gather(f32[1,1,128]{2,1,0:T(1,128)S(1)} %bitcast.40), channel_id=1, replica_groups=mesh['fs'=16,'tp'=2] {'fs'}, dimensions={0}, use_global_device_ids=true | all-gather | bytes 8704 | tf_op jit(solution)/shard_map/all_gather | solution.py:47
  55.1 1.5 fusion.7
  56.7 35.8 %all-gather.15.cloned.1.call-done = bf16[2048,768]{1,0:T(8,128)(2,1)} async-done(((bf16[128,768]{1,0:T(8,128)(2,1)}), bf16[2048,768]{1,0:T(8,128)(2,1)}) %all-gather.15.cloned.1.call-update) | async-done | bytes 3145744 | tf_op jit(solution)/shard_map/all_gather | solution.py:58
  92.5 3.5 multiply_reduce_fusion
  96.0 2.6 psum.14
  98.6 0.1 multiply_convert_fusion
  98.8 0.2 copy.30
  99.0 0.1 reshape.46
  99.1 0.4 fusion.11
  99.5 0.6 copy.32
  100.1 0.1 copy.40
  100.2 0.3 copy.33
  100.4 61.3 %all-gather.13.cloned.1.call-done = bf16[2048,768]{1,0:T(8,128)(2,1)} async-done(((bf16[128,768]{1,0:T(8,128)(2,1)}), bf16[2048,768]{1,0:T(8,128)(2,1)}) %all-gather.13.cloned.1.call-update) | async-done | bytes 3145744 | tf_op jit(solution)/shard_map/all_gather | solution.py:57
  161.7 77.2 %all-gather.17.cloned.1.call-done = bf16[768,2048]{1,0:T(8,128)(2,1)} async-done(((bf16[768,128]{1,0:T(8,128)(2,1)}), bf16[768,2048]{1,0:T(8,128)(2,1)}) %all-gather.17.cloned.1.call-update) | async-done | bytes 3145744 | tf_op jit(solution)/shard_map/all_gather | solution.py:84
  238.9 6.2 fusion.3
  245.2 1.0 convert_element_type.77
  246.2 2.4 convert_element_type.74
  248.7 0.9 convert_element_type.75
  249.7 38.3 %all-gather.2 = f32[16,1,128]{2,1,0:T(1,128)S(1)} all-gather(f32[1,1,128]{2,1,0:T(1,128)S(1)} %bitcast.41), channel_id=1, replica_groups=mesh['fs'=16,'tp'=2] {'fs'}, dimensions={0}, use_global_device_ids=true | all-gather | bytes 8704 | tf_op jit(solution)/shard_map/all_gather | solution.py:48
  288.0 1.7 fusion.4
  289.8 118.3 %all-gather.23.cloned.1.call-done = bf16[45056,128]{1,0:T(8,128)(2,1)} async-done(((bf16[2816,128]{1,0:T(8,128)(2,1)}), bf16[45056,128]{1,0:T(8,128)(2,1)}) %all-gather.23.cloned.1.call-update) | async-done | bytes 11534352 | tf_op jit(solution)/shard_map/all_gather | solution.py:104
  408.1 15.2 %copy.34 = bf16[2816,16,128]{0,2,1:T(8,128)(2,1)} copy(bf16[2816,16,128]{2,0,1:T(8,128)(2,1)} %bitcast.33) | data formatting | bytes 23068672 | tf_op jit(solution)/shard_map/reshape | solution.py:104
  423.3 127.2 %all-gather.19.cloned.1.call-done = bf16[2048,2816]{1,0:T(8,128)(2,1)} async-done(((bf16[128,2816]{1,0:T(8,128)(2,1)}), bf16[2048,2816]{1,0:T(8,128)(2,1)}) %all-gather.19.cloned.1.call-update) | async-done | bytes 11534352 | tf_op jit(solution)/shard_map/all_gather | solution.py:93
  550.5 9.1 %convolution_multiply_fusion.1 = f32[256,2816]{1,0:T(8,128)} fusion(bf16[2048,2816]{1,0:T(8,128)(2,1)} %all-gather.19.cloned.1.call-done, f32[2816]{0:T(1024)S(1)} %copy-done.8, bf16[256,2048]{1,0:T(8,128)(2,1)S(1)} %get-tuple-element.6, f32[2048]{0:T(1024)S(1)} %copy-done.11, f32[256]{0:T(256)S(1)} %add_rsqrt_fusion), kind=kOutput, calls=%fused_computation.2 | convolution fusion | flops 2955608064 | bytes 15486976 | tf_op jit(solution)/shard_map/dot_general | solution.py:96
  559.6 133.3 %all-gather.21.cloned.1.call-done = bf16[2048,2816]{1,0:T(8,128)(2,1)} async-done(((bf16[128,2816]{1,0:T(8,128)(2,1)}), bf16[2048,2816]{1,0:T(8,128)(2,1)}) %all-gather.21.cloned.1.call-update) | async-done | bytes 11534352 | tf_op jit(solution)/shard_map/all_gather | solution.py:94
  692.9 15.7 %fusion.2 = bf16[256,2048]{1,0:T(8,128)(2,1)} fusion(bf16[2816,2048]{0,1:T(8,128)(2,1)} %bitcast.34, f32[2048]{0:T(1024)S(1)} %bitcast.39, bf16[2048,2816]{1,0:T(8,128)(2,1)} %all-gather.21.cloned.1.call-done, f32[256,2816]{1,0:T(8,128)} %convolution_multiply_fusion.1, f32[2816]{0:T(1024)S(1)} %copy-done.9, bf16[256,2048]{1,0:T(8,128)(2,1)S(1)} %get-tuple-element.6, ...), kind=kOutput, calls=%fused_computation.11 | convolution fusion | flops 5913772032 | bytes 28078080 | tf_op jit(solution)/shard_map/dot_general | solution.py:23
  708.6 6.7 reduce-scatter.2.cloned.1.call-done
  715.3 2.0 add_convert_fusion
  (51 shorter events, 0.6 us)
Async XLA Ops:
  6.5 6.1 copy-start.6
  6.5 86.0 %copy-start.10 = (f32[2048]{0:T(1024)S(1)}, f32[2048]{0:T(1024)}, u32[]{:S(2)}) copy-start(f32[2048]{0:T(1024)} %param.19) | copy-start | bytes 24580
  6.5 86.0 %copy-start.12 = (f32[768]{0:T(1024)S(1)}, f32[768]{0:T(1024)}, u32[]{:S(2)}) copy-start(f32[768]{0:T(1024)} %param.23) | copy-start | bytes 9220
  6.5 48.6 %all-gather.11.cloned.1.call-start = ((), (), s32[]{:S(2)}) async-start(), calls=%async_computation.1 | async-start | bytes 1572864 | tf_op jit(solution)/shard_map/all_gather | solution.py:50
  7.3 85.3 %all-gather.15.cloned.1.call-start = ((), (), s32[]{:S(2)}) async-start(), calls=%async_computation.3 | async-start | bytes 3342336 | tf_op jit(solution)/shard_map/all_gather | solution.py:58
  9.0 152.7 %all-gather.13.cloned.1.call-start = ((), (), s32[]{:S(2)}) async-start(), calls=%async_computation.2 | async-start | bytes 3342336 | tf_op jit(solution)/shard_map/all_gather | solution.py:57
  10.8 228.1 %all-gather.17.cloned.1.call-start = ((), (), s32[]{:S(2)}) async-start(), calls=%async_computation.4 | async-start | bytes 3342336 | tf_op jit(solution)/shard_map/all_gather | solution.py:84
  12.6 275.5 %all-reduce.2.cloned.1.call-start = ((), (), s32[]{:S(2)}) async-start(), calls=%async_computation.5 | async-start | bytes 2097152 | tf_op jit(solution)/shard_map/psum | solution.py:86
  56.7 42.0 %copy-start.5 = (f32[768]{0:T(1024)S(1)}, f32[768]{0:T(1024)}, u32[]{:S(2)}) copy-start(f32[768]{0:T(1024)} %param.24) | copy-start | bytes 9220
  56.7 42.4 %copy-start.4 = (f32[12,128]{1,0:T(8,128)S(1)}, f32[12,128]{1,0:T(8,128)}, u32[]{:S(2)}) copy-start(f32[12,128]{1,0:T(8,128)} %param.26) | copy-start | bytes 18436
  96.0 3.1 copy-start.3
  99.1 139.8 %copy-start = (bf16[256,2048]{1,0:T(8,128)(2,1)S(1)}, bf16[256,2048]{1,0:T(8,128)(2,1)}, u32[]{:S(2)}) copy-start(bf16[256,2048]{1,0:T(8,128)(2,1)} %all-gather.11.cloned.1.call-done) | copy-start | bytes 3145732
  99.1 139.8 %copy-start.13 = (f32[768]{0:T(1024)S(1)}, f32[768]{0:T(1024)}, u32[]{:S(2)}) copy-start(f32[768]{0:T(1024)} %param.21) | copy-start | bytes 9220
  238.9 6.2 copy-start.1
  245.1 163.0 %all-gather.23.cloned.1.call-start = ((), (), s32[]{:S(2)}) async-start(), calls=%async_computation.9 | async-start | bytes 12255232 | tf_op jit(solution)/shard_map/all_gather | solution.py:104
  246.1 2.6 copy-start.2
  246.2 3.6 copy-start.7
  246.2 304.3 %all-gather.19.cloned.1.call-start = ((), (), s32[]{:S(2)}) async-start(), calls=%async_computation.6 | async-start | bytes 12255232 | tf_op jit(solution)/shard_map/all_gather | solution.py:93
  248.7 444.3 %all-gather.21.cloned.1.call-start = ((), (), s32[]{:S(2)}) async-start(), calls=%async_computation.7 | async-start | bytes 12255232 | tf_op jit(solution)/shard_map/all_gather | solution.py:94
  249.7 465.6 %reduce-scatter.2.cloned.1.call-start = ((), (), s32[]{:S(2)}) async-start(), calls=%async_computation.8 | async-start | bytes 1572864 | tf_op jit(solution)/shard_map/reduce_scatter | solution.py:106
  408.1 142.4 %copy-start.8 = (f32[2816]{0:T(1024)S(1)}, f32[2816]{0:T(1024)}, u32[]{:S(2)}) copy-start(f32[2816]{0:T(1024)} %param.31) | copy-start | bytes 33796
  408.1 142.4 %copy-start.11 = (f32[2048]{0:T(1024)S(1)}, f32[2048]{0:T(1024)}, u32[]{:S(2)}) copy-start(f32[2048]{0:T(1024)} %param.29) | copy-start | bytes 24580
  550.5 142.4 %copy-start.9 = (f32[2816]{0:T(1024)S(1)}, f32[2816]{0:T(1024)}, u32[]{:S(2)}) copy-start(f32[2816]{0:T(1024)} %param.33) | copy-start | bytes 33796
Sparse Core Ops, SparseCore 0:
  8.9 11.7 all-gather.10
  23.4 69.0 all-gather.14
  95.3 66.3 all-gather.12
  164.3 74.5 all-gather.16
  245.2 17.5 all-reduce.1
  265.5 142.6 all-gather.22
  410.9 139.5 all-gather.18
  553.3 139.6 all-gather.20
  708.7 6.5 reduce-scatter.1
